TPU v7x, 32 devices: a whole 2x2x4 slice. The times are simulated.
32 devices in a mesh: ep: 32 (over z, y, x, core).
Axes of the slice: x: 2, y: 2, z: 4, core: 2. Of those that a mesh axis runs over, the one named last changes fastest.
Arguments:
- tokens: bfloat16 [768, 2048], P('ep'), may hold values from -6 to 6
- state: float32 [768, 16, 64, 64], P('ep'), may hold values from -4 to 4
- norm_gain: float32 [2048], replicated, may hold values from 0.1 to 1.9
- w_recept: bfloat16 [2048, 1024], replicated, may hold values from -0.125 to 0.125
- w_keys: bfloat16 [2048, 1024], replicated, may hold values from -0.125 to 0.125
- w_values: bfloat16 [2048, 1024], replicated, may hold values from -0.125 to 0.125
- decay_base: float32 [1024], replicated, may hold values from -3 to 3
- decay_first_matrix: bfloat16 [2048, 128], replicated, may hold values from -0.125 to 0.125
- decay_second_matrix: bfloat16 [128, 1024], replicated, may hold values from -0.5 to 0.5
- rate_base: float32 [1024], replicated, may hold values from -3 to 3
- rate_first_matrix: bfloat16 [2048, 128], replicated, may hold values from -0.125 to 0.125
- rate_second_matrix: bfloat16 [128, 1024], replicated, may hold values from -0.5 to 0.5
- head_gain: float32 [1024], replicated, may hold values from 0.1 to 1.9
- w_output: bfloat16 [1024, 2048], replicated, may hold values from -0.1875 to 0.1875
- second_gain: float32 [2048], replicated, may hold values from 0.1 to 1.9
- route_ids: int32 [768, 2], replicated, may hold values from 0 to 15, all different within a row; in each aligned block of 24 rows (0 to 23, 24 to 47, ...) at most 6 rows name the same one
- route_weights: float32 [768, 2], replicated, may hold values from 0.2 to 1
- expert_gate: bfloat16 [2048, 49152], P(None, 'ep'), may hold values from -0.125 to 0.125
- expert_up: bfloat16 [2048, 49152], P(None, 'ep'), may hold values from -0.125 to 0.125
- expert_down: bfloat16 [49152, 2048], P('ep'), may hold values from -0.109375 to 0.109375
Outputs:
- layer_out: bfloat16 [768, 2048], P('ep')
- new_state: float32 [768, 16, 64, 64], P('ep')
Inputs may be any that keep to these rules, and one draw needn't show every extreme that they name: `route_ids`: each row names 2 different experts. Among the 24 rows of one device (aligned blocks), no expert is named by more than 6 rows, and in every draw some block names some expert exactly 6 times.
All inputs are finite; a program needn't handle non-finite values.
Results may differ from a plain program's by a relative error of at most 0.015.
Values may be sent and summed in bfloat16 or wider, within the bound.
A program may use at most 192 MiB of HBM per device.

v0:
```python
import jax
import jax.numpy as jnp
from jax import lax
from jax.sharding import PartitionSpec as P

EXPERTS = 16
CAP_DEV = 6


def norm_rows(values, gain):
    mean_sq = jnp.mean(values * values, axis=-1, keepdims=True)
    return values * lax.rsqrt(mean_sq + 1e-06) * gain


def time_mixer(
    tokens,
    state,
    norm_gain,
    w_recept,
    w_keys,
    w_values,
    decay_base,
    decay_first_matrix,
    decay_second_matrix,
    rate_base,
    rate_first_matrix,
    rate_second_matrix,
    head_gain,
    w_output,
):
    count = tokens.shape[0]
    heads = state.shape[1]
    width = state.shape[2]
    resid = tokens.astype(jnp.float32)
    normed = norm_rows(resid, norm_gain).astype(jnp.bfloat16)
    recept = jnp.dot(normed, w_recept, preferred_element_type=jnp.float32).astype(jnp.bfloat16)
    keys = jnp.dot(normed, w_keys, preferred_element_type=jnp.float32).astype(jnp.bfloat16)
    vals = jnp.dot(normed, w_values, preferred_element_type=jnp.float32).astype(jnp.bfloat16)
    decay_low = jnp.tanh(
        jnp.dot(normed, decay_first_matrix, preferred_element_type=jnp.float32)
    ).astype(jnp.bfloat16)
    rate_low = jnp.dot(normed, rate_first_matrix, preferred_element_type=jnp.float32).astype(
        jnp.bfloat16
    )
    pre = decay_base + jnp.dot(decay_low, decay_second_matrix, preferred_element_type=jnp.float32)
    decay = jnp.exp(-jnp.exp(-jax.nn.softplus(-pre) - 0.5))
    rate = jax.nn.sigmoid(
        rate_base + jnp.dot(rate_low, rate_second_matrix, preferred_element_type=jnp.float32)
    )

    def split_heads(values):
        return values.astype(jnp.float32).reshape(count, heads, width)

    r_head = split_heads(recept)
    k_head = split_heads(keys)
    v_head = split_heads(vals)
    d_head = split_heads(decay)
    a_head = split_heads(rate)
    unit = k_head * lax.rsqrt(jnp.sum(k_head * k_head, axis=-1, keepdims=True) + 1e-06)
    probe = jnp.einsum("bhvk,bhk->bhv", state, unit, precision=lax.Precision.HIGHEST)
    updated = (
        state * d_head[:, :, None, :]
        - probe[..., None] * (unit * a_head)[:, :, None, :]
        + v_head[..., None] * k_head[:, :, None, :]
    )
    mixed = jnp.einsum("bhvk,bhk->bhv", updated, r_head, precision=lax.Precision.HIGHEST)
    centre = mixed - jnp.mean(mixed, axis=-1, keepdims=True)
    spread = jnp.mean(centre * centre, axis=-1, keepdims=True)
    mixed = centre * lax.rsqrt(spread + 0.00064)
    mixed = (mixed.reshape(count, heads * width) * head_gain).astype(jnp.bfloat16)
    after = resid + jnp.dot(mixed, w_output, preferred_element_type=jnp.float32)
    return (after, updated)


def expert_part(rows, gate_w, up_w, down_w):
    gate = jnp.dot(rows, gate_w, preferred_element_type=jnp.float32)
    upper = jnp.dot(rows, up_w, preferred_element_type=jnp.float32)
    hidden = (jax.nn.silu(gate) * upper).astype(jnp.bfloat16)
    return jnp.dot(hidden, down_w, preferred_element_type=jnp.float32)


def slot_table(member, slots):
    order = jnp.cumsum(member.astype(jnp.int32), axis=1) - 1
    match = order[:, None, :] == jnp.arange(slots, dtype=jnp.int32)[None, :, None]
    return (match & member[:, None, :]).astype(jnp.float32)


def on_device(
    tokens,
    state,
    norm_gain,
    w_recept,
    w_keys,
    w_values,
    decay_base,
    decay_first_matrix,
    decay_second_matrix,
    rate_base,
    rate_first_matrix,
    rate_second_matrix,
    head_gain,
    w_output,
    second_gain,
    route_ids,
    route_weights,
    expert_gate,
    expert_up,
    expert_down,
):
    after, new_state = time_mixer(
        tokens,
        state,
        norm_gain,
        w_recept,
        w_keys,
        w_values,
        decay_base,
        decay_first_matrix,
        decay_second_matrix,
        rate_base,
        rate_first_matrix,
        rate_second_matrix,
        head_gain,
        w_output,
    )
    second = norm_rows(after, second_gain).astype(jnp.bfloat16)
    devices = lax.axis_size("ep")
    group = devices // EXPERTS
    rows_dev = tokens.shape[0]
    slots = CAP_DEV
    width = tokens.shape[1]
    start = lax.axis_index("ep") * rows_dev
    own_ids = lax.dynamic_slice_in_dim(route_ids, start, rows_dev, 0)
    own_weights = lax.dynamic_slice_in_dim(route_weights, start, rows_dev, 0)
    hit = own_ids[None, :, :] == jnp.arange(EXPERTS, dtype=jnp.int32)[:, None, None]
    member = jnp.any(hit, axis=2)
    share = jnp.sum(jnp.where(hit, own_weights[None, :, :], 0.0), axis=2)
    table = slot_table(member, slots)
    packed = jnp.einsum(
        "ecs,sf->ecf", table.astype(jnp.bfloat16), second, preferred_element_type=jnp.float32
    ).astype(jnp.bfloat16)
    outgoing = jnp.repeat(packed, group, axis=0)
    received = lax.all_to_all(outgoing, "ep", split_axis=0, concat_axis=0, tiled=True)
    count = received.shape[1]
    partial_value = expert_part(
        received.reshape(devices * count, width), expert_gate, expert_up, expert_down
    )
    returned = lax.all_to_all(
        partial_value.reshape(devices, count, width).astype(jnp.bfloat16),
        "ep",
        split_axis=0,
        concat_axis=0,
        tiled=True,
    ).astype(jnp.float32)
    summed = jnp.sum(returned.reshape(EXPERTS, group, slots, width), axis=1)
    blend = jnp.einsum(
        "ecs,ecf->sf", table * share[:, None, :], summed, precision=lax.Precision.HIGHEST
    )
    layer_out = (after + blend).astype(jnp.bfloat16)
    return (layer_out, new_state)


def solution(mesh):
    in_specs = (
        P("ep", None),
        P("ep", None, None, None),
        P(),
        P(),
        P(),
        P(),
        P(),
        P(),
        P(),
        P(),
        P(),
        P(),
        P(),
        P(),
        P(),
        P(),
        P(),
        P(None, "ep"),
        P(None, "ep"),
        P("ep", None),
    )
    out_specs = (P("ep", None), P("ep", None, None, None))
    return jax.shard_map(
        on_device, mesh=mesh, in_specs=in_specs, out_specs=out_specs, check_vma=False
    )
```

profile of v0, /device:TPU:0, one launch (start us, length us, event | category | flops | bytes accessed | tf_op | source)
XLA Modules:
  0.0 139.8 jit_solution(11655732401048659084)
XLA Ops:
  0.6 0.0 copy-start
  0.6 0.0 copy-start.3
  0.7 0.0 copy-start.6
  0.7 0.0 copy-start.8
  0.7 0.0 copy-start.4
  0.7 0.0 copy-start.5
  0.7 1.1 fusion.13
  1.8 3.0 %fusion.9 = f32[24,1024]{1,0:T(8,128)S(1)} fusion(bf16[2048,1024]{1,0:T(8,128)(2,1)} %param.24, bf16[24,2048]{1,0:T(8,128)(2,1)} %param.20, f32[2048]{0:T(1024)} %param.22, f32[24]{0:T(128)S(1)} %add_rsqrt_fusion.3), kind=kOutput, calls=%fused_computation.21 | convolution fusion | flops 100909056 | bytes 4399200 | tf_op jit(solution)/shard_map/dot_general | solution.py:37
  4.8 0.1 reshape.109
  4.9 0.1 multiply_reduce_fusion.2
  5.1 0.0 copy-done
  5.1 1.4 %fusion.7 = f32[24,1024]{1,0:T(8,128)S(1)} fusion(bf16[128,1024]{1,0:T(8,128)(2,1)} %param.31, bf16[2048,128]{1,0:T(8,128)(2,1)S(1)} %copy-done, f32[1024]{0:T(1024)} %param.29, bf16[24,2048]{1,0:T(8,128)(2,1)} %param.20, f32[2048]{0:T(1024)} %param.22, f32[24]{0:T(128)S(1)} %add_rsqrt_fusion.3), kind=kOutput, calls=%fused_computation.16 | convolution fusion | flops 19172352 | bytes 995424 | tf_op jit(solution)/shard_map/dot_general | solution.py:48
  6.5 0.1 reshape.101
  6.6 0.0 copy-done.3
  6.6 0.0 copy-done.6
  6.6 0.5 fusion.22
  7.1 0.1 mul.143
  7.2 2.9 %fusion.8 = f32[24,1024]{1,0:T(8,128)S(1)} fusion(bf16[2048,1024]{1,0:T(8,128)(2,1)} %param.25, bf16[24,2048]{1,0:T(8,128)(2,1)S(1)} %copy-done.3, f32[2048]{0:T(1024)S(1)} %copy-done.6, f32[24]{0:T(128)S(1)} %add_rsqrt_fusion.3), kind=kOutput, calls=%fused_computation.19 | convolution fusion | flops 100909056 | bytes 4399200 | tf_op jit(solution)/shard_map/dot_general | solution.py:38
  10.1 0.1 reshape.110
  10.2 2.9 %convolution_convert_fusion.2 = bf16[24,1024]{1,0:T(8,128)(2,1)S(1)} fusion(bf16[2048,1024]{1,0:T(8,128)(2,1)} %param.23, bf16[24,2048]{1,0:T(8,128)(2,1)S(1)} %copy-done.3, f32[2048]{0:T(1024)S(1)} %copy-done.6, f32[24]{0:T(128)S(1)} %add_rsqrt_fusion.3), kind=kOutput, calls=%fused_computation.17 | convolution fusion | flops 100884480 | bytes 4350048 | tf_op jit(solution)/shard_map/dot_general | solution.py:36
  13.1 0.2 reshape.120
  13.2 0.1 fusion.45
  13.4 22.0 %fusion.46 = f32[24,16,1,64]{3,2,1,0:T(1,128)S(1)} fusion(f32[24,16,64,1]{2,3,1,0:T(1,128)S(1)} %bitcast.42, f32[24,16,64,64]{3,2,1,0:T(8,128)} %param.21), kind=kOutput, calls=%fused_computation.73 | convolution fusion | flops 18874368 | bytes 6488064 | tf_op jit(solution)/shard_map/bhvk,bhk->bhv/dot_general | solution.py:60
  35.4 9.8 %multiply_add_fusion = f32[24,16,64,64]{3,2,1,0:T(8,128)S(1)} fusion(f32[24,16,64,64]{3,2,1,0:T(8,128)} %param.21, f32[24,16,64]{2,1,0:T(8,128)S(1)} %reshape.109, f32[24,16,64]{2,1,0:T(8,128)S(1)} %reshape.110, f32[24,16,64]{2,1,0:T(8,128)S(1)} %get-tuple-element.2, f32[24,16,64]{2,1,0:T(8,128)S(1)} %bitcast.41, f32[24,16,64]{2,1,0:T(8,128)S(1)} %mul.143), kind=kLoop, calls=%fused_computation | loop fusion | flops 7864320 | bytes 13074432 | tf_op jit(solution)/shard_map/add | solution.py:62
  45.2 0.0 copy-start.2
  45.3 0.0 copy-start.9
  45.3 0.0 copy-start.7
  45.3 9.9 %fusion.47 = f32[24,16,1,64]{3,2,1,0:T(1,128)S(1)} fusion(f32[24,16,64,64]{3,2,1,0:T(8,128)S(1)} %multiply_add_fusion, bf16[24,16,64,1]{2,3,1,0:T(2,128)(2,1)S(1)} %reshape.120), kind=kOutput, calls=%fused_computation.74 | convolution fusion | flops 18874368 | bytes 6438912 | tf_op jit(solution)/shard_map/bhvk,bhk->bhv/dot_general | solution.py:66
  55.1 0.1 reduce_sum.65
  55.3 0.2 multiply_reduce_fusion.1
  55.5 0.2 subtract_multiply_fusion
  55.7 0.1 reshape.103
  55.8 3.0 %multiply_reduce_fusion = (f32[24]{0:T(128)S(1)}, f32[24,2048]{1,0:T(8,128)S(1)}) fusion(bf16[1024,2048]{1,0:T(8,128)(2,1)} %param.33, f32[24,1024]{1,0:T(8,128)S(1)} %reshape.103, f32[1024]{0:T(1024)S(1)} %copy-done.9, bf16[24,2048]{1,0:T(8,128)(2,1)S(1)} %copy-done.3), kind=kOutput, calls=%fused_computation.34 | convolution fusion | flops 100909032 | bytes 4591712 | tf_op jit(solution)/shard_map/dot_general | solution.py:71
  58.8 0.8 constant_dynamic-slice_fusion.1
  59.6 0.2 reduce_window_sum.11
  59.8 0.3 convolution_convert_fusion.1
  60.1 0.2 copy.32
  60.3 0.1 broadcast_in_dim.12
  60.4 33.3 %all_to_all.10 = bf16[32,6,2048]{2,1,0:T(8,128)(2,1)S(1)} all-to-all(bf16[32,6,2048]{2,1,0:T(8,128)(2,1)S(1)} %bitcast.37), channel_id=1, replica_groups=mesh['ep'=32] {'ep'}, dimensions={0} | all-to-all | bytes 1572864 | tf_op jit(solution)/shard_map/all_to_all | solution.py:143
  93.8 0.3 reshape.105
  94.0 5.2 %fusion.48 = f32[192,1536]{1,0:T(8,128)} fusion(bf16[192,2048]{1,0:T(8,128)(2,1)S(1)} %reshape.105, bf16[2048,1536]{1,0:T(8,128)(2,1)} %param.37), kind=kOutput, calls=%fused_computation.75 | convolution fusion | flops 1207959552 | bytes 8257536 | tf_op jit(solution)/shard_map/dot_general | solution.py:76
  99.2 7.7 %convolution_convert_fusion = bf16[192,2048]{1,0:T(8,128)(2,1)S(1)} fusion(bf16[1536,2048]{1,0:T(8,128)(2,1)} %param.39, bf16[192,2048]{1,0:T(8,128)(2,1)S(1)} %reshape.105, bf16[2048,1536]{1,0:T(8,128)(2,1)} %param.38, f32[192,1536]{1,0:T(8,128)} %fusion.48), kind=kOutput, calls=%fused_computation.3 | convolution fusion | flops 2418081792 | bytes 15335424 | tf_op jit(solution)/shard_map/dot_general | solution.py:79
  106.9 1.2 convert_element_type.74
  108.1 3.6 %all-to-all-start.1 = ((bf16[32,6,2048]{2,1,0:T(8,128)(2,1)}), bf16[32,6,2048]{2,1,0:T(8,128)(2,1)S(1)}, u32[]{:S(2)}, u32[]{:S(2)}) async-start(bf16[32,6,2048]{2,1,0:T(8,128)(2,1)} %convert_element_type.74), calls=%async_computation.1 | async-start | bytes 2097152 | tf_op jit(solution)/shard_map/all_to_all | solution.py:148
  111.8 0.8 constant_dynamic-slice_fusion
  112.6 25.4 %all-to-all-done.1 = bf16[32,6,2048]{2,1,0:T(8,128)(2,1)S(1)} async-done(((bf16[32,6,2048]{2,1,0:T(8,128)(2,1)}), bf16[32,6,2048]{2,1,0:T(8,128)(2,1)S(1)}, u32[]{:S(2)}, u32[]{:S(2)}) %all-to-all-start.1) | async-done | bytes 786464 | tf_op jit(solution)/shard_map/all_to_all | solution.py:148
  138.0 0.2 convert_reduce_fusion
  138.2 1.6 %fusion.2 = bf16[24,2048]{1,0:T(8,128)(2,1)} fusion(f32[24,2048]{1,0:T(8,128)S(1)} %get-tuple-element.5, f32[16,6,2048]{2,1,0:T(8,128)S(1)} %convert_reduce_fusion, f32[16,24]{1,0:T(8,128)S(1)} %select_reduce_fusion, s32[16,24]{1,0:T(8,128)S(1)} %broadcast_add_fusion, pred[16,24]{1,0:T(8,128)(4,1)S(1)} %fusion.35), kind=kOutput, calls=%fused_computation.8 | convolution fusion | flops 56728320 | bytes 1084800 | tf_op jit(solution)/shard_map/ecs,ecf->sf/dot_general | solution.py:156
  (17 shorter events, 0.1 us)
Async XLA Ops:
  0.6 4.4 %copy-start = (bf16[2048,128]{1,0:T(8,128)(2,1)S(1)}, bf16[2048,128]{1,0:T(8,128)(2,1)}, u32[]{:S(2)}) copy-start(bf16[2048,128]{1,0:T(8,128)(2,1)} %param.30) | copy-start | bytes 1572868
  0.6 5.9 %copy-start.3 = (bf16[24,2048]{1,0:T(8,128)(2,1)S(1)}, bf16[24,2048]{1,0:T(8,128)(2,1)}, u32[]{:S(2)}) copy-start(bf16[24,2048]{1,0:T(8,128)(2,1)} %param.20) | copy-start | bytes 294916
  0.7 5.9 %copy-start.6 = (f32[2048]{0:T(1024)S(1)}, f32[2048]{0:T(1024)}, u32[]{:S(2)}) copy-start(f32[2048]{0:T(1024)} %param.22) | copy-start | bytes 24580
  0.7 5.9 %copy-start.8 = (f32[1024]{0:T(1024)S(1)}, f32[1024]{0:T(1024)}, u32[]{:S(2)}) copy-start(f32[1024]{0:T(1024)} %param.26) | copy-start | bytes 12292
  0.7 5.9 %copy-start.4 = (bf16[2048,128]{1,0:T(8,128)(2,1)S(1)}, bf16[2048,128]{1,0:T(8,128)(2,1)}, u32[]{:S(2)}) copy-start(bf16[2048,128]{1,0:T(8,128)(2,1)} %param.27) | copy-start | bytes 1572868
  0.7 5.9 %copy-start.5 = (bf16[128,1024]{1,0:T(8,128)(2,1)S(1)}, bf16[128,1024]{1,0:T(8,128)(2,1)}, u32[]{:S(2)}) copy-start(bf16[128,1024]{1,0:T(8,128)(2,1)} %param.28) | copy-start | bytes 786436
  45.2 9.9 %copy-start.2 = (f32[24,16,64,64]{3,2,1,0:T(8,128)}, f32[24,16,64,64]{3,2,1,0:T(8,128)S(1)}, u32[]{:S(2)}) copy-start(f32[24,16,64,64]{3,2,1,0:T(8,128)S(1)} %multiply_add_fusion) | copy-start | bytes 18874372
  45.3 10.6 %copy-start.9 = (f32[1024]{0:T(1024)S(1)}, f32[1024]{0:T(1024)}, u32[]{:S(2)}) copy-start(f32[1024]{0:T(1024)} %param.32) | copy-start | bytes 12292
  45.3 14.5 %copy-start.7 = (f32[2048]{0:T(1024)S(1)}, f32[2048]{0:T(1024)}, u32[]{:S(2)}) copy-start(f32[2048]{0:T(1024)} %param.34) | copy-start | bytes 24580
  99.2 40.6 %copy-start.1 = (bf16[2048,128]{1,0:T(8,128)(2,1)S(1)}, bf16[2048,128]{1,0:T(8,128)(2,1)}, u32[]{:S(2)}) copy-start(bf16[2048,128]{1,0:T(8,128)(2,1)} %param.30) | copy-start | bytes 1572868
  108.1 29.8 %all-to-all-start.1 = ((bf16[32,6,2048]{2,1,0:T(8,128)(2,1)}), bf16[32,6,2048]{2,1,0:T(8,128)(2,1)S(1)}, u32[]{:S(2)}, u32[]{:S(2)}) async-start(bf16[32,6,2048]{2,1,0:T(8,128)(2,1)} %convert_element_type.74), calls=%async_computation.1 | async-start | bytes 2097152 | tf_op jit(solution)/shard_map/all_to_all | solution.py:148
where the time goes:
time: 140 us
  matrix products  60.2 us (43%)
  blocking collectives  33.3 us (24%)
  waiting for transfers between devices  25.4 us (18%)
  other arithmetic  12.2 us (9%)
  local copies, waits for them, and re-layouts  4.1 us (3%)
  starting transfers between devices  3.63 us (3%)
    all_to_all x1, blocking collectives, on_device(): lax.all_to_all(outgoing, 'ep', split_axis=0, concat_axis=0, tiled=True)  33.3 us
    all_to_all x1, waiting for transfers between devices, on_device(): lax.all_to_all(partial_value.reshape(devices, count, width).astype(jnp.bf...  25.4 us
    dot_general x1, matrix products, time_mixer(): jnp.einsum('bhvk,bhk->bhv', state, unit, precision=lax.Precision.HIGHEST)  22 us
    dot_general x1, matrix products, time_mixer(): jnp.einsum('bhvk,bhk->bhv', updated, r_head, precision=lax.Precision.HIGH...  9.85 us
    add x1, other arithmetic, time_mixer(): state * d_head[:, :, None, :]  9.85 us
    dot_general x1, matrix products, expert_part(): return jnp.dot(hidden, down_w, preferred_element_type=jnp.float32)  7.66 us
    dot_general x1, matrix products, expert_part(): gate = jnp.dot(rows, gate_w, preferred_element_type=jnp.float32)  5.18 us
    all_to_all x1, starting transfers between devices, on_device(): lax.all_to_all(partial_value.reshape(devices, count, width).astype(jnp.bf...  3.63 us
  transfers between devices with their start and end apart: 1, of which 1 were waited for; matrix products, arithmetic and copies ran while one was open for 1% of the time, Pallas kernels for 0%

commit v1 on v0

v1 whole, which is shorter than its diff:
```python
import functools
import math

import jax
import jax.numpy as jnp
from jax import lax
from jax.experimental import pallas as pl
from jax.experimental.pallas import tpu as pltpu
from jax.sharding import PartitionSpec as P

EXPERTS = 16
CAP_DEV = 6
ROWS = 8
PARTS = 3
MESH = pl.DeviceIdType.MESH
BF = jnp.bfloat16
F32 = jnp.float32


def dot(a, b):
    return jnp.dot(a, b, preferred_element_type=F32)


def mixer_kernel(
    tokens, norm_gain, decay_base, rate_base, head_gain, second_gain, table,
    state, w_recept, w_keys, w_values, d_first, d_second, r_first, r_second, w_output,
    new_state, after_ref, packed_ref,
    st, wr, wk, wv, df, ds, rf, rs, wo, kh, rh, dh, ah, vt, mt,
    w_sem, in_sem, out_sem,
):
    count, heads, width, _ = state.shape
    loads = [
        pltpu.make_async_copy(src, dst, w_sem.at[i])
        for i, (src, dst) in enumerate(
            [
                (d_first, df), (r_first, rf), (w_keys, wk), (w_values, wv), (d_second, ds),
                (r_second, rs), (w_recept, wr), (w_output, wo),
            ]
        )
    ]
    for copy in loads[:7]:
        copy.start()

    def fetch(h):
        return pltpu.make_async_copy(state.at[:, h], st.at[h], in_sem.at[h])

    def put(h):
        return pltpu.make_async_copy(st.at[h], new_state.at[:, h], out_sem.at[h])

    def start_fetch(h, c):
        fetch(h).start()
        return c

    lax.fori_loop(0, heads, start_fetch, 0)
    loads[7].start()

    resid = tokens[...].astype(F32)
    mean_sq = jnp.mean(resid * resid, axis=-1, keepdims=True)
    normed = (resid * lax.rsqrt(mean_sq + 1e-06) * norm_gain[...]).astype(BF)

    def spread(ref, values):
        for h in range(heads):
            ref[h] = values[:, h * width:(h + 1) * width]

    loads[0].wait()
    decay_low = jnp.tanh(dot(normed, df[...])).astype(BF)
    loads[1].wait()
    rate_low = dot(normed, rf[...]).astype(BF)
    loads[2].wait()
    spread(kh, dot(normed, wk[...]).astype(BF).astype(F32))
    loads[3].wait()
    vals = dot(normed, wv[...]).astype(BF).astype(F32)
    lanes = vt.shape[1]
    vt[...] = jnp.concatenate(
        [vals, jnp.zeros((lanes - count, vals.shape[1]), F32)], axis=0
    ).T
    loads[4].wait()
    pre = decay_base[...] + dot(decay_low, ds[...])
    spread(dh, jnp.exp(-jax.nn.sigmoid(pre) * math.exp(-0.5)))
    loads[5].wait()
    spread(ah, jax.nn.sigmoid(rate_base[...] + dot(rate_low, rs[...])))
    loads[6].wait()
    spread(rh, dot(normed, wr[...]).astype(BF).astype(F32))

    def one_head(h, c):
        fetch(h).wait()
        k = kh[h]
        r = rh[h]
        d = dh[h]
        unit = k * lax.rsqrt(jnp.sum(k * k, axis=-1, keepdims=True) + 1e-06)
        ua = unit * ah[h]
        rows = pl.ds(pl.multiple_of(h * width, width), width)
        v = vt[rows, :]
        lane = lax.broadcasted_iota(jnp.int32, (width, lanes), 1)
        mixed = jnp.zeros((width, lanes), F32)
        for b in range(count):
            s = st[h, b]
            probe = jnp.sum(s * unit[b:b + 1], axis=-1, keepdims=True)
            new = s * d[b:b + 1] - probe * ua[b:b + 1] + v[:, b:b + 1] * k[b:b + 1]
            st[h, b] = new
            got = jnp.sum(new * r[b:b + 1], axis=-1, keepdims=True)
            mixed = jnp.where(lane == b, got, mixed)
        put(h).start()
        centre = mixed - jnp.mean(mixed, axis=0, keepdims=True)
        var = jnp.mean(centre * centre, axis=0, keepdims=True)
        mt[rows, :] = centre * lax.rsqrt(var + 0.00064)
        return c

    lax.fori_loop(0, heads, one_head, 0)
    mixed = (mt[...].T[:count] * head_gain[...]).astype(BF)
    loads[7].wait()
    after = resid + dot(mixed, wo[...])
    after_ref[...] = after
    mean_sq = jnp.mean(after * after, axis=-1, keepdims=True)
    second = (after * lax.rsqrt(mean_sq + 1e-06) * second_gain[...]).astype(BF)
    part = second.shape[1] // (PARTS + 1)
    last = second[:, PARTS * part:]
    for j in range(PARTS):
        value = dot(table[PARTS], second[:, j * part:(j + 1) * part]) + dot(table[j], last)
        packed_ref[:, :, j * part:(j + 1) * part] = value.reshape(EXPERTS, ROWS, part).astype(BF)

    def end_put(h, c):
        put(h).wait()
        return c

    lax.fori_loop(0, heads, end_put, 0)


def mixer(args, table):
    (tokens, state, norm_gain, w_recept, w_keys, w_values, decay_base, d_first, d_second,
     rate_base, r_first, r_second, head_gain, w_output, second_gain) = args
    count, heads, width, _ = state.shape
    model = tokens.shape[1]
    part = model // (PARTS + 1)
    lanes = -(-count // 128) * 128
    vm = pl.BlockSpec(memory_space=pltpu.VMEM)
    hb = pl.BlockSpec(memory_space=pl.ANY)
    weights = [w_recept, w_keys, w_values, d_first, d_second, r_first, r_second, w_output]
    head_buf = pltpu.VMEM((heads, count, width), F32)
    return pl.pallas_call(
        mixer_kernel,
        out_shape=(
            jax.ShapeDtypeStruct(state.shape, F32),
            jax.ShapeDtypeStruct((count, model), F32),
            jax.ShapeDtypeStruct((EXPERTS, ROWS, PARTS * part), BF),
        ),
        in_specs=[vm] * 7 + [hb] * 9,
        out_specs=(hb, vm, vm),
        scratch_shapes=[
            pltpu.VMEM((heads, count, width, width), F32),
            *[pltpu.VMEM(w.shape, w.dtype) for w in weights],
            head_buf, head_buf, head_buf, head_buf,
            pltpu.VMEM((heads * width, lanes), F32),
            pltpu.VMEM((heads * width, lanes), F32),
            pltpu.SemaphoreType.DMA((8,)),
            pltpu.SemaphoreType.DMA((heads,)),
            pltpu.SemaphoreType.DMA((heads,)),
        ],
        compiler_params=pltpu.CompilerParams(vmem_limit_bytes=56 * 1024 * 1024),
        name="mixer",
    )(
        tokens, norm_gain[None], decay_base[None], rate_base[None], head_gain[None],
        second_gain[None], table, state, *weights,
    )


def expert_kernel(
    devices, packed, after, blend_w, unpack_m, pack_m, gate_h, up_h, down_h,
    out_ref,
    buf, rows_x, hidden, part_f, part_b, peer_b, zsend, ret, gate, up, down,
    w_sem, send1, recv1, fsend, frecv, ysend, yrecv, rsend, rrecv, own_sem,
):
    group = devices // EXPERTS
    me = lax.axis_index("ep")
    mine = me // group
    place = lax.rem(me, group)
    model = after.shape[1]
    part = model // (PARTS + 1)
    inner = gate.shape[1]
    step = math.gcd(inner, 256)

    loads = [
        pltpu.make_async_copy(src, dst, w_sem.at[i])
        for i, (src, dst) in enumerate([(gate_h, gate), (up_h, up), (down_h, down)])
    ]
    barrier = pltpu.get_barrier_semaphore()

    def other(i):
        return lax.rem(mine + i, EXPERTS)

    def peer(i):
        return lax.rem(place + i, group)

    def greet(i, c):
        pl.semaphore_signal(
            barrier, inc=1, device_id=(other(i) * group + place,), device_id_type=MESH
        )
        return c

    lax.fori_loop(1, EXPERTS, greet, 0)
    for i in range(1, group):
        pl.semaphore_signal(
            barrier, inc=1, device_id=(mine * group + peer(i),), device_id_type=MESH
        )
    for copy in loads:
        copy.start()
    pl.semaphore_wait(barrier, EXPERTS - 1 + group - 1)

    def dispatch(i):
        e = other(i)
        return pltpu.make_async_remote_copy(
            src_ref=packed.at[e], dst_ref=buf.at[place, mine],
            send_sem=send1.at[e], recv_sem=recv1.at[mine],
            device_id=(e * group + place,), device_id_type=MESH,
        )

    def arrive(s):
        return pltpu.make_async_remote_copy(
            src_ref=packed.at[s], dst_ref=buf.at[place, s],
            send_sem=send1.at[s], recv_sem=recv1.at[s],
            device_id=(s * group + place,), device_id_type=MESH,
        )

    def forward(s, i, src):
        q = peer(i)
        return pltpu.make_async_remote_copy(
            src_ref=src, dst_ref=buf.at[place, s],
            send_sem=fsend.at[i, s], recv_sem=frecv.at[place, s],
            device_id=(mine * group + q,), device_id_type=MESH,
        )

    def forwarded(s, i):
        q = peer(i)
        return pltpu.make_async_remote_copy(
            src_ref=buf.at[q, s], dst_ref=buf.at[q, s],
            send_sem=fsend.at[i, s], recv_sem=frecv.at[q, s],
            device_id=(mine * group + q,), device_id_type=MESH,
        )

    def start_dispatch(i, c):
        dispatch(i).start()
        return c

    lax.fori_loop(1, EXPERTS, start_dispatch, 0)
    own = pltpu.make_async_copy(packed.at[mine], buf.at[place, mine], own_sem.at[0])
    own.start()
    for i in range(1, group):
        forward(mine, i, packed.at[mine]).start()

    def relay(j, c):
        s = lax.rem(mine + EXPERTS - j, EXPERTS)
        arrive(s).wait_recv()
        for i in range(1, group):
            forward(s, i, buf.at[place, s]).start()
        return c

    lax.fori_loop(1, EXPERTS, relay, 0)
    own.wait()

    def end_relay(j, c):
        s = lax.rem(mine + EXPERTS - j, EXPERTS)
        for i in range(1, group):
            forwarded(s, i).wait_recv()
        return c

    lax.fori_loop(0, EXPERTS, end_relay, 0)

    packed_rows = EXPERTS * ROWS
    rows = EXPERTS * CAP_DEV
    for q in range(group):
        tail = jnp.zeros((rows, part), F32)
        for j in range(PARTS):
            cols = slice(j * part, (j + 1) * part)
            block = buf[q, :, :, cols].astype(F32).reshape(packed_rows, part).astype(BF)
            rows_x[q * rows:(q + 1) * rows, cols] = dot(unpack_m[PARTS], block).astype(BF)
            tail = tail + dot(unpack_m[j], block)
        rows_x[q * rows:(q + 1) * rows, PARTS * part:] = tail.astype(BF)

    loads[0].wait()
    loads[1].wait()

    def up_step(t, c):
        cols = pl.ds(pl.multiple_of(t * step, step), step)
        g = dot(rows_x[...], gate[:, cols])
        u = dot(rows_x[...], up[:, cols])
        hidden[:, cols] = (g * jax.nn.sigmoid(g) * u).astype(BF)
        return c

    lax.fori_loop(0, inner // step, up_step, 0)
    loads[2].wait()
    wide = math.gcd(model, 256)

    def down_step(t, c):
        cols = pl.ds(pl.multiple_of(t * wide, wide), wide)
        y = dot(hidden[...], down[:, cols])
        for q in range(group):
            mine_rows = y[q * rows:(q + 1) * rows]
            part_f[q, :, cols] = mine_rows
            part_b[q, :, cols] = mine_rows.astype(BF)
        return c

    lax.fori_loop(0, model // wide, down_step, 0)

    def swap(i):
        q = peer(i)
        return pltpu.make_async_remote_copy(
            src_ref=part_b.at[q], dst_ref=peer_b.at[place],
            send_sem=ysend.at[q], recv_sem=yrecv.at[place],
            device_id=(mine * group + q,), device_id_type=MESH,
        )

    def swapped(i):
        q = peer(i)
        return pltpu.make_async_remote_copy(
            src_ref=part_b.at[q], dst_ref=peer_b.at[q],
            send_sem=ysend.at[q], recv_sem=yrecv.at[q],
            device_id=(mine * group + q,), device_id_type=MESH,
        )

    for i in range(1, group):
        swap(i).start()
    for i in range(1, group):
        swapped(i).wait_recv()

    def summed(cols):
        total = part_f[place, :, cols]
        for i in range(1, group):
            total = total + peer_b[peer(i), :, cols].astype(F32)
        return total.astype(BF)

    last = summed(slice(PARTS * part, model))
    for j in range(PARTS):
        cols = slice(j * part, (j + 1) * part)
        value = dot(pack_m[PARTS], summed(cols)) + dot(pack_m[j], last)
        zsend[:, :, cols] = value.reshape(EXPERTS, ROWS, part).astype(BF)

    def give(i):
        e = other(i)
        return pltpu.make_async_remote_copy(
            src_ref=zsend.at[e], dst_ref=ret.at[mine],
            send_sem=rsend.at[e], recv_sem=rrecv.at[mine],
            device_id=(e * group + place,), device_id_type=MESH,
        )

    def take(s):
        return pltpu.make_async_remote_copy(
            src_ref=zsend.at[s], dst_ref=ret.at[s],
            send_sem=rsend.at[s], recv_sem=rrecv.at[s],
            device_id=(s * group + place,), device_id_type=MESH,
        )

    def start_give(i, c):
        give(i).start()
        return c

    lax.fori_loop(1, EXPERTS, start_give, 0)
    own_back = pltpu.make_async_copy(zsend.at[mine], ret.at[mine], own_sem.at[1])
    own_back.start()

    def drain(i, c):
        dispatch(i).wait_send()
        s = lax.rem(mine + EXPERTS - i, EXPERTS)
        for k in range(1, group):
            forwarded(s, k).wait_send()
        return c

    lax.fori_loop(1, EXPERTS, drain, 0)
    for i in range(1, group):
        forwarded(mine, i).wait_send()
        swap(i).wait_send()
    own_back.wait()

    def end_take(j, c):
        take(lax.rem(mine + EXPERTS - j, EXPERTS)).wait_recv()
        return c

    lax.fori_loop(1, EXPERTS, end_take, 0)

    high = blend_w[...].astype(BF)
    low = (blend_w[...] - high.astype(F32)).astype(BF)
    tail = after[:, PARTS * part:]
    for j in range(PARTS):
        cols = slice(j * part, (j + 1) * part)
        block = ret[:, :, cols].astype(F32).reshape(packed_rows, part).astype(BF)
        value = after[:, cols] + dot(high[PARTS], block) + dot(low[PARTS], block)
        out_ref[:, cols] = value.astype(BF)
        tail = tail + dot(high[j], block) + dot(low[j], block)
    out_ref[:, PARTS * part:] = tail.astype(BF)

    def end_give(i, c):
        give(i).wait_send()
        return c

    lax.fori_loop(1, EXPERTS, end_give, 0)


def experts(packed, after, blend_w, gate, up, down, devices):
    group = devices // EXPERTS
    count, model = after.shape
    inner = gate.shape[1]
    rows = EXPERTS * CAP_DEV
    row = jnp.arange(rows)[:, None]
    place = jnp.arange(EXPERTS * ROWS)[None, :]
    same = row // CAP_DEV == place // ROWS
    slot, at = row % CAP_DEV, place % ROWS
    maps = [
        same & (at == CAP_DEV + slot // PARTS) & (slot % PARTS == j) for j in range(PARTS)
    ] + [same & (at == slot)]
    unpack_m = jnp.stack(maps).astype(BF)
    pack_m = unpack_m.transpose(0, 2, 1)
    vm = pl.BlockSpec(memory_space=pltpu.VMEM)
    hb = pl.BlockSpec(memory_space=pl.ANY)
    wide = packed.shape[2]
    dma = pltpu.SemaphoreType.DMA
    return pl.pallas_call(
        functools.partial(expert_kernel, devices),
        out_shape=jax.ShapeDtypeStruct((count, model), BF),
        in_specs=[vm] * 5 + [hb] * 3,
        out_specs=vm,
        scratch_shapes=[
            pltpu.VMEM((group, EXPERTS, ROWS, wide), BF),
            pltpu.VMEM((group * rows, model), BF),
            pltpu.VMEM((group * rows, inner), BF),
            pltpu.VMEM((group, rows, model), F32),
            pltpu.VMEM((group, rows, model), BF),
            pltpu.VMEM((group, rows, model), BF),
            pltpu.VMEM((EXPERTS, ROWS, wide), BF),
            pltpu.VMEM((EXPERTS, ROWS, wide), BF),
            pltpu.VMEM(gate.shape, BF),
            pltpu.VMEM(up.shape, BF),
            pltpu.VMEM(down.shape, BF),
            dma((3,)),
            dma((EXPERTS,)),
            dma((EXPERTS,)),
            dma((group, EXPERTS)),
            dma((group, EXPERTS)),
            dma((group,)),
            dma((group,)),
            dma((EXPERTS,)),
            dma((EXPERTS,)),
            dma((2,)),
        ],
        compiler_params=pltpu.CompilerParams(
            collective_id=0, has_side_effects=True, vmem_limit_bytes=56 * 1024 * 1024
        ),
        name="experts",
    )(packed, after, blend_w, unpack_m, pack_m, gate, up, down)


def tables(route_ids, route_weights, rows_dev):
    start = lax.axis_index("ep") * rows_dev
    ids = lax.dynamic_slice_in_dim(route_ids, start, rows_dev, 0)
    weights = lax.dynamic_slice_in_dim(route_weights, start, rows_dev, 0)
    hit = ids[None, :, :] == jnp.arange(EXPERTS, dtype=jnp.int32)[:, None, None]
    member = jnp.any(hit, axis=2)
    share = jnp.sum(jnp.where(hit, weights[None, :, :], 0.0), axis=2)
    order = jnp.cumsum(member.astype(jnp.int32), axis=1) - 1
    order = jnp.where(member, order, -1)[None, :, None, :]
    at = jnp.arange(ROWS, dtype=jnp.int32)[None, None, :, None]
    piece = jnp.arange(PARTS + 1, dtype=jnp.int32)[:, None, None, None]
    base = jnp.where(
        piece == PARTS,
        jnp.where(at < CAP_DEV, at, -2),
        jnp.where(at >= CAP_DEV, (at - CAP_DEV) * PARTS + piece, -2),
    )
    table = (order == base).astype(F32)
    blend = table * share[None, :, None, :]
    flat = (PARTS + 1, EXPERTS * ROWS, rows_dev)
    return table.reshape(flat).astype(BF), blend.reshape(flat).transpose(0, 2, 1)


def on_device(
    tokens, state, norm_gain, w_recept, w_keys, w_values, decay_base, decay_first_matrix,
    decay_second_matrix, rate_base, rate_first_matrix, rate_second_matrix, head_gain, w_output,
    second_gain, route_ids, route_weights, expert_gate, expert_up, expert_down,
):
    devices = lax.axis_size("ep")
    table, blend_w = tables(route_ids, route_weights, tokens.shape[0])
    new_state, after, packed = mixer(
        (tokens, state, norm_gain, w_recept, w_keys, w_values, decay_base, decay_first_matrix,
         decay_second_matrix, rate_base, rate_first_matrix, rate_second_matrix, head_gain,
         w_output, second_gain),
        table,
    )
    layer_out = experts(packed, after, blend_w, expert_gate, expert_up, expert_down, devices)
    return (layer_out, new_state)


def solution(mesh):
    rep = P()
    in_specs = (
        P("ep", None), P("ep", None, None, None), *[rep] * 15,
        P(None, "ep"), P(None, "ep"), P("ep", None),
    )
    out_specs = (P("ep", None), P("ep", None, None, None))
    return jax.shard_map(
        on_device, mesh=mesh, in_specs=in_specs, out_specs=out_specs, check_vma=False
    )
```

time: 140 us -> 92.5 us (0.66)
  Pallas kernels: 0 us -> 84.6 us
  matrix products: 60.2 us -> 0 us
  blocking collectives: 33.3 us -> 0 us
  waiting for transfers between devices: 25.4 us -> 0 us
  other arithmetic: 12.2 us -> 2.62 us
  starting transfers between devices: 3.63 us -> 0 us
    pallas_call x0 -> x2, Pallas kernels: none -> 84.6 us  [the longest x1 47.7 us: mixer(): pl.pallas_call(mixer_kernel, out_shape=(jax.ShapeDtypeStruct(state.shape,...]
    dot_general x12 -> x0, matrix products: 60.2 us -> none  [the longest x1 22 us: time_mixer(): jnp.einsum('bhvk,bhk->bhv', state, unit, precision=lax.Precision.HIGHEST)]
    all_to_all x1 -> x0, blocking collectives: 33.3 us -> none  [on_device(): lax.all_to_all(outgoing, 'ep', split_axis=0, concat_axis=0, tiled=True)]
    all_to_all x1 -> x0, waiting for transfers between devices: 25.4 us -> none  [on_device(): lax.all_to_all(partial_value.reshape(devices, count, width).astype(jnp.bf...]
    add x1, other arithmetic: 9.85 us -> 0.02 us  [experts(): CAP_DEV + slot // PARTS]
    all_to_all x1 -> x0, starting transfers between devices: 3.63 us -> none  [on_device(): lax.all_to_all(partial_value.reshape(devices, count, width).astype(jnp.bf...]
    unnamed x20 -> x3, local copies, waits for them, and re-layouts: 0.06 us -> 2.16 us
    reduce_sum x6 -> x1, other arithmetic: 1.83 us -> 0.01 us  [tables(): share = jnp.sum(jnp.where(hit, weights[None, :, :], 0.0), axis=2)]
  transfers between devices with their start and end apart: 1 -> 0, of which waited for: 1 -> 0; matrix products, arithmetic and copies ran while one was open for 1% -> 0% of each run, Pallas kernels for 0% -> 0%
where the time goes in v1:
time: 92.5 us; the launch traced here: 91.9 us
  Pallas kernels  84.6 us (91%)
  local copies, waits for them, and re-layouts  3.95 us (4%)
  other arithmetic  2.62 us (3%)
    pallas_call x1, Pallas kernels, mixer(): pl.pallas_call(mixer_kernel, out_shape=(jax.ShapeDtypeStruct(state.shape,...  47.7 us
    pallas_call x1, Pallas kernels, experts(): pl.pallas_call(functools.partial(expert_kernel, devices), out_shape=jax.S...  36.9 us
    unnamed x3, local copies, waits for them, and re-layouts  2.16 us

profile of v1, /device:TPU:0, one launch (start us, length us, event | category | flops | bytes accessed | tf_op | source)
XLA Modules:
  0.0 91.9 jit_solution(10735843760182928607)
XLA Ops:
  0.6 0.0 copy-start
  0.7 0.6 copy-done
  1.3 0.1 constant_dynamic-slice_fusion.1
  1.4 0.8 constant_dynamic-slice_fusion
  2.2 0.1 select_select_fusion
  2.3 0.2 reduce_window_sum.11
  2.5 0.1 eq.227
  2.6 0.1 copy.36
  2.7 0.1 fusion.2
  2.8 0.1 copy.35
  2.9 0.6 compare_select_fusion.blend_w
  3.5 0.8 convert_convert_fusion.table
  4.3 0.7 fusion.5
  5.0 0.7 copy.38.unpack_m
  5.7 47.7 %mixer.1 = (f32[24,16,64,64]{3,2,1,0:T(8,128)}, f32[24,2048]{1,0:T(8,128)}, bf16[16,8,1536]{2,1,0:T(8,128)(2,1)}) custom-call(bf16[24,2048]{1,0:T(8,128)(2,1)} %tokens.1, f32[1,2048]{1,0:T(1,128)} %bitcast.16, f32[1,1024]{1,0:T(1,128)} %bitcast.18, f32[1,1024]{1,0:T(1,128)} %bitcast.19, f32[1,1024]{1,0:T(1,128)} %bitcast.20, f32[1,2048]{1,0:T(1,128)} %bitcast.17, ...), custom_call_target="tpu_custom_call" | custom-call | tf_op jit(solution)/shard_map/mixer/pallas_call | solution.py:140
  53.4 36.9 %experts.1 = bf16[24,2048]{1,0:T(8,128)(2,1)} custom-call(bf16[16,8,1536]{2,1,0:T(8,128)(2,1)} %get-tuple-element.5.packed, f32[24,2048]{1,0:T(8,128)} %get-tuple-element.6.after, f32[4,24,128]{2,1,0:T(8,128)} %compare_select_fusion.blend_w, bf16[4,96,128]{2,1,0:T(8,128)(2,1)} %copy.38.unpack_m, bf16[4,128,96]{2,1,0:T(8,128)(2,1)} %get-tuple-element.8.pack_m, ...), custom_call_target="tpu_custom_call" | custom-call | tf_op jit(solution)/shard_map/experts/pallas_call | solution.py:415
  90.4 1.5 %copy.40 = bf16[24,2048]{1,0:T(8,128)(2,1)} copy(bf16[24,2048]{1,0:T(8,128)(2,1)} %experts.1) | data formatting | bytes 196608
  (15 shorter events, 0.1 us)
Async XLA Ops:
  0.6 0.7 copy-start

commit v2 on v1

--- a/solution.py
+++ b/solution.py
@@ -3,6 +3,7 @@
 
 import jax
 import jax.numpy as jnp
+import numpy as np
 from jax import lax
 from jax.experimental import pallas as pl
 from jax.experimental.pallas import tpu as pltpu
@@ -25,7 +26,7 @@
     tokens, norm_gain, decay_base, rate_base, head_gain, second_gain, table,
     state, w_recept, w_keys, w_values, d_first, d_second, r_first, r_second, w_output,
     new_state, after_ref, packed_ref,
-    st, wr, wk, wv, df, ds, rf, rs, wo, kh, rh, dh, ah, vt, mt,
+    st, wr, wk, wv, df, ds, rf, rs, wo, kh, dh, ah, vt, rt, mt,
     w_sem, in_sem, out_sem,
 ):
     count, heads, width, _ = state.shape
@@ -51,8 +52,9 @@
         fetch(h).start()
         return c
 
-    lax.fori_loop(0, heads, start_fetch, 0)
-    loads[7].start()
+    def start_fetches(turn_at):
+        low, high = turn_at * heads // 3, (turn_at + 1) * heads // 3
+        lax.fori_loop(low, high, start_fetch, 0)
 
     resid = tokens[...].astype(F32)
     mean_sq = jnp.mean(resid * resid, axis=-1, keepdims=True)
@@ -61,6 +63,12 @@
     def spread(ref, values):
         for h in range(heads):
             ref[h] = values[:, h * width:(h + 1) * width]
+
+    lanes = vt.shape[1]
+
+    def turn(values):
+        blank = jnp.zeros((lanes - count, values.shape[1]), F32)
+        return jnp.concatenate([values, blank], axis=0).T
 
     loads[0].wait()
     decay_low = jnp.tanh(dot(normed, df[...])).astype(BF)
@@ -68,38 +76,57 @@
     rate_low = dot(normed, rf[...]).astype(BF)
     loads[2].wait()
     spread(kh, dot(normed, wk[...]).astype(BF).astype(F32))
+    start_fetches(0)
     loads[3].wait()
     vals = dot(normed, wv[...]).astype(BF).astype(F32)
-    lanes = vt.shape[1]
-    vt[...] = jnp.concatenate(
-        [vals, jnp.zeros((lanes - count, vals.shape[1]), F32)], axis=0
-    ).T
+    vt[...] = turn(vals)
+    start_fetches(1)
     loads[4].wait()
     pre = decay_base[...] + dot(decay_low, ds[...])
     spread(dh, jnp.exp(-jax.nn.sigmoid(pre) * math.exp(-0.5)))
     loads[5].wait()
     spread(ah, jax.nn.sigmoid(rate_base[...] + dot(rate_low, rs[...])))
     loads[6].wait()
-    spread(rh, dot(normed, wr[...]).astype(BF).astype(F32))
+    rt[...] = turn(dot(normed, wr[...]).astype(BF).astype(F32))
+    start_fetches(2)
+    loads[7].start()
+
+    block = math.gcd(count, 8)
+    ones = jnp.ones((width, width), BF)
+    lane = lax.broadcasted_iota(jnp.int32, (width, lanes), 1)
+
+    def dot_split(values, right):
+        flat = values.reshape(-1, values.shape[-1])
+        high = flat.astype(BF)
+        low = (flat - high.astype(F32)).astype(BF)
+        return dot(high, right) + dot(low, right)
 
     def one_head(h, c):
         fetch(h).wait()
         k = kh[h]
-        r = rh[h]
         d = dh[h]
         unit = k * lax.rsqrt(jnp.sum(k * k, axis=-1, keepdims=True) + 1e-06)
         ua = unit * ah[h]
         rows = pl.ds(pl.multiple_of(h * width, width), width)
         v = vt[rows, :]
-        lane = lax.broadcasted_iota(jnp.int32, (width, lanes), 1)
+        r = rt[rows, :].astype(BF)
+        tall = jnp.concatenate([k, jnp.zeros((lanes - count, width), F32)], axis=0).astype(BF)
         mixed = jnp.zeros((width, lanes), F32)
-        for b in range(count):
-            s = st[h, b]
-            probe = jnp.sum(s * unit[b:b + 1], axis=-1, keepdims=True)
-            new = s * d[b:b + 1] - probe * ua[b:b + 1] + v[:, b:b + 1] * k[b:b + 1]
-            st[h, b] = new
-            got = jnp.sum(new * r[b:b + 1], axis=-1, keepdims=True)
-            mixed = jnp.where(lane == b, got, mixed)
+        for g in range(count // block):
+            some = range(g * block, (g + 1) * block)
+
+            def each(values):
+                return jnp.stack([jnp.broadcast_to(values[b:b + 1], (width, width)) for b in some])
+
+            s = st[h, g * block:(g + 1) * block]
+            probe = dot_split(s * each(unit), ones).reshape(block, width, width)
+            masked = jnp.concatenate([jnp.where(lane == b, v, 0.0) for b in some], axis=0)
+            outer = dot(masked.astype(BF), tall).reshape(block, width, width)
+            new = s * each(d) - probe * each(ua) + outer
+            st[h, g * block:(g + 1) * block] = new
+            got = dot_split(new, r).reshape(block, width, lanes)
+            for i, b in enumerate(some):
+                mixed = jnp.where(lane == b, got[i], mixed)
         put(h).start()
         centre = mixed - jnp.mean(mixed, axis=0, keepdims=True)
         var = jnp.mean(centre * centre, axis=0, keepdims=True)
@@ -149,7 +176,8 @@
         scratch_shapes=[
             pltpu.VMEM((heads, count, width, width), F32),
             *[pltpu.VMEM(w.shape, w.dtype) for w in weights],
-            head_buf, head_buf, head_buf, head_buf,
+            head_buf, head_buf, head_buf,
+            pltpu.VMEM((heads * width, lanes), F32),
             pltpu.VMEM((heads * width, lanes), F32),
             pltpu.VMEM((heads * width, lanes), F32),
             pltpu.SemaphoreType.DMA((8,)),
@@ -399,15 +427,16 @@
     count, model = after.shape
     inner = gate.shape[1]
     rows = EXPERTS * CAP_DEV
-    row = jnp.arange(rows)[:, None]
-    place = jnp.arange(EXPERTS * ROWS)[None, :]
+    row = np.arange(rows)[:, None]
+    place = np.arange(EXPERTS * ROWS)[None, :]
     same = row // CAP_DEV == place // ROWS
     slot, at = row % CAP_DEV, place % ROWS
     maps = [
         same & (at == CAP_DEV + slot // PARTS) & (slot % PARTS == j) for j in range(PARTS)
     ] + [same & (at == slot)]
-    unpack_m = jnp.stack(maps).astype(BF)
-    pack_m = unpack_m.transpose(0, 2, 1)
+    maps = np.stack(maps).astype(np.float32)
+    unpack_m = jnp.asarray(maps, BF)
+    pack_m = jnp.asarray(maps.transpose(0, 2, 1), BF)
     vm = pl.BlockSpec(memory_space=pltpu.VMEM)
     hb = pl.BlockSpec(memory_space=pl.ANY)
     wide = packed.shape[2]
@@ -456,13 +485,13 @@
     share = jnp.sum(jnp.where(hit, weights[None, :, :], 0.0), axis=2)
     order = jnp.cumsum(member.astype(jnp.int32), axis=1) - 1
     order = jnp.where(member, order, -1)[None, :, None, :]
-    at = jnp.arange(ROWS, dtype=jnp.int32)[None, None, :, None]
-    piece = jnp.arange(PARTS + 1, dtype=jnp.int32)[:, None, None, None]
-    base = jnp.where(
+    at = np.arange(ROWS)[None, None, :, None]
+    piece = np.arange(PARTS + 1)[:, None, None, None]
+    base = np.where(
         piece == PARTS,
-        jnp.where(at < CAP_DEV, at, -2),
-        jnp.where(at >= CAP_DEV, (at - CAP_DEV) * PARTS + piece, -2),
-    )
+        np.where(at < CAP_DEV, at, -2),
+        np.where(at >= CAP_DEV, (at - CAP_DEV) * PARTS + piece, -2),
+    ).astype(np.int32)
     table = (order == base).astype(F32)
     blend = table * share[None, :, None, :]
     flat = (PARTS + 1, EXPERTS * ROWS, rows_dev)

time: 92.5 us -> 71.1 us (0.77)
  Pallas kernels: 84.6 us -> 64.3 us
  other arithmetic: 2.62 us -> 1.63 us
    pallas_call x1, Pallas kernels: 47.7 us -> 27.3 us  [mixer(): pl.pallas_call(mixer_kernel, out_shape=(jax.ShapeDtypeStruct(state.shape,...]
where the time goes in v2:
time: 71.1 us; the launch traced here: 70.6 us
  Pallas kernels  64.3 us (90%)
  local copies, waits for them, and re-layouts  3.96 us (6%)
  other arithmetic  1.63 us (2%)
    pallas_call x1, Pallas kernels, experts(): pl.pallas_call(functools.partial(expert_kernel, devices), out_shape=jax.S...  37 us
    pallas_call x1, Pallas kernels, mixer(): pl.pallas_call(mixer_kernel, out_shape=(jax.ShapeDtypeStruct(state.shape,...  27.3 us
    unnamed x3, local copies, waits for them, and re-layouts  2.23 us

profile of v2, /device:TPU:0, one launch (start us, length us, event | category | flops | bytes accessed | tf_op | source)
XLA Modules:
  0.0 70.6 jit_solution(11411626836371571476)
XLA Ops:
  0.6 0.0 copy-start
  0.6 0.7 copy-done
  1.3 0.1 constant_dynamic-slice_fusion.1
  1.4 0.8 %constant_dynamic-slice_fusion = f32[24,2]{0,1:T(2,128)S(1)} fusion(f32[768,2]{0,1:T(2,128)} %param.39, s32[]{:T(128)S(6)} %select_n.16), kind=kLoop, calls=%fused_computation.9 | loop fusion | bytes 388 | tf_op jit(solution)/shard_map/dynamic_slice | solution.py:482
  2.2 0.2 reduce_window_sum.11
  2.4 0.7 eq.54
  3.1 0.1 eq.55
  3.2 0.1 copy.34
  3.2 0.1 copy.33
  3.3 0.7 compare_select_fusion.blend_w
  3.9 0.8 %convert_convert_fusion.table = bf16[4,128,24]{2,1,0:T(8,128)(2,1)} fusion(s32[4,128]{1,0:T(4,128)S(1)} %eq.55, s32[128,24]{1,0:T(8,128)S(1)} %get-tuple-element.9), kind=kLoop, calls=%fused_computation | loop fusion | flops 36864 | bytes 38912 | tf_op jit(solution)/shard_map/convert_element_type | solution.py:498
  4.7 27.3 %mixer.1 = (f32[24,16,64,64]{3,2,1,0:T(8,128)}, f32[24,2048]{1,0:T(8,128)}, bf16[16,8,1536]{2,1,0:T(8,128)(2,1)}) custom-call(bf16[24,2048]{1,0:T(8,128)(2,1)} %tokens.1, f32[1,2048]{1,0:T(1,128)} %bitcast.14, f32[1,1024]{1,0:T(1,128)} %bitcast.16, f32[1,1024]{1,0:T(1,128)} %bitcast.17, f32[1,1024]{1,0:T(1,128)} %bitcast.18, f32[1,2048]{1,0:T(1,128)} %bitcast.15, ...), custom_call_target="tpu_custom_call" | custom-call | tf_op jit(solution)/shard_map/mixer/pallas_call | solution.py:167
  32.0 37.0 %experts.1 = bf16[24,2048]{1,0:T(8,128)(2,1)} custom-call(bf16[16,8,1536]{2,1,0:T(8,128)(2,1)} %get-tuple-element.5.packed, f32[24,2048]{1,0:T(8,128)} %get-tuple-element.6.after, f32[4,24,128]{2,1,0:T(8,128)} %compare_select_fusion.blend_w, bf16[4,96,128]{2,1,0:T(8,128)(2,1)} %constant.29.clone.unpack_m, bf16[4,128,96]{2,1,0:T(8,128)(2,1)} %constant.30.clone.pack_m, ...), custom_call_target="tpu_custom_call" | custom-call | tf_op jit(solution)/shard_map/experts/pallas_call | solution.py:444
  69.1 1.5 %copy.36 = bf16[24,2048]{1,0:T(8,128)(2,1)} copy(bf16[24,2048]{1,0:T(8,128)(2,1)} %experts.1) | data formatting | bytes 196608
  (6 shorter events, 0.1 us)
Async XLA Ops:
  0.6 0.7 copy-start

commit v3 on v2

--- a/solution.py
+++ b/solution.py
@@ -23,9 +23,9 @@
 
 
 def mixer_kernel(
-    tokens, norm_gain, decay_base, rate_base, head_gain, second_gain, table,
+    tokens, norm_gain, decay_base, rate_base, head_gain, second_gain, order, share,
     state, w_recept, w_keys, w_values, d_first, d_second, r_first, r_second, w_output,
-    new_state, after_ref, packed_ref,
+    new_state, after_ref, packed_ref, blend_ref,
     st, wr, wk, wv, df, ds, rf, rs, wo, kh, dh, ah, vt, rt, mt,
     w_sem, in_sem, out_sem,
 ):
@@ -55,6 +55,20 @@
     def start_fetches(turn_at):
         low, high = turn_at * heads // 3, (turn_at + 1) * heads // 3
         lax.fori_loop(low, high, start_fetch, 0)
+
+    shape = (EXPERTS, ROWS, count)
+    slot = jnp.broadcast_to(order[...][:, None, :], shape)
+    weight = jnp.broadcast_to(share[...][:, None, :], shape)
+    at = lax.broadcasted_iota(jnp.int32, shape, 1)
+    table = []
+    for j in range(PARTS + 1):
+        if j == PARTS:
+            hits = (slot == at) & (at < CAP_DEV)
+        else:
+            hits = (slot == (at - CAP_DEV) * PARTS + j) & (at >= CAP_DEV)
+        hits = jnp.where(hits, 1.0, 0.0)
+        blend_ref[j] = (hits * weight).reshape(EXPERTS * ROWS, count)
+        table.append(hits.reshape(EXPERTS * ROWS, count).astype(BF))
 
     resid = tokens[...].astype(F32)
     mean_sq = jnp.mean(resid * resid, axis=-1, keepdims=True)
@@ -153,7 +167,7 @@
     lax.fori_loop(0, heads, end_put, 0)
 
 
-def mixer(args, table):
+def mixer(args, order, share):
     (tokens, state, norm_gain, w_recept, w_keys, w_values, decay_base, d_first, d_second,
      rate_base, r_first, r_second, head_gain, w_output, second_gain) = args
     count, heads, width, _ = state.shape
@@ -170,9 +184,10 @@
             jax.ShapeDtypeStruct(state.shape, F32),
             jax.ShapeDtypeStruct((count, model), F32),
             jax.ShapeDtypeStruct((EXPERTS, ROWS, PARTS * part), BF),
+            jax.ShapeDtypeStruct((PARTS + 1, EXPERTS * ROWS, count), F32),
         ),
-        in_specs=[vm] * 7 + [hb] * 9,
-        out_specs=(hb, vm, vm),
+        in_specs=[vm] * 8 + [hb] * 9,
+        out_specs=(hb, vm, vm, vm),
         scratch_shapes=[
             pltpu.VMEM((heads, count, width, width), F32),
             *[pltpu.VMEM(w.shape, w.dtype) for w in weights],
@@ -188,7 +203,7 @@
         name="mixer",
     )(
         tokens, norm_gain[None], decay_base[None], rate_base[None], head_gain[None],
-        second_gain[None], table, state, *weights,
+        second_gain[None], order, share, state, *weights,
     )
 
 
@@ -404,15 +419,18 @@
 
     lax.fori_loop(1, EXPERTS, end_take, 0)
 
+    def dot_turned(left, right):
+        return lax.dot_general(left, right, (((0,), (0,)), ((), ())), preferred_element_type=F32)
+
     high = blend_w[...].astype(BF)
     low = (blend_w[...] - high.astype(F32)).astype(BF)
     tail = after[:, PARTS * part:]
     for j in range(PARTS):
         cols = slice(j * part, (j + 1) * part)
         block = ret[:, :, cols].astype(F32).reshape(packed_rows, part).astype(BF)
-        value = after[:, cols] + dot(high[PARTS], block) + dot(low[PARTS], block)
+        value = after[:, cols] + dot_turned(high[PARTS], block) + dot_turned(low[PARTS], block)
         out_ref[:, cols] = value.astype(BF)
-        tail = tail + dot(high[j], block) + dot(low[j], block)
+        tail = tail + dot_turned(high[j], block) + dot_turned(low[j], block)
     out_ref[:, PARTS * part:] = tail.astype(BF)
 
     def end_give(i, c):
@@ -484,18 +502,7 @@
     member = jnp.any(hit, axis=2)
     share = jnp.sum(jnp.where(hit, weights[None, :, :], 0.0), axis=2)
     order = jnp.cumsum(member.astype(jnp.int32), axis=1) - 1
-    order = jnp.where(member, order, -1)[None, :, None, :]
-    at = np.arange(ROWS)[None, None, :, None]
-    piece = np.arange(PARTS + 1)[:, None, None, None]
-    base = np.where(
-        piece == PARTS,
-        np.where(at < CAP_DEV, at, -2),
-        np.where(at >= CAP_DEV, (at - CAP_DEV) * PARTS + piece, -2),
-    ).astype(np.int32)
-    table = (order == base).astype(F32)
-    blend = table * share[None, :, None, :]
-    flat = (PARTS + 1, EXPERTS * ROWS, rows_dev)
-    return table.reshape(flat).astype(BF), blend.reshape(flat).transpose(0, 2, 1)
+    return jnp.where(member, order, -1), share
 
 
 def on_device(
@@ -504,12 +511,13 @@
     second_gain, route_ids, route_weights, expert_gate, expert_up, expert_down,
 ):
     devices = lax.axis_size("ep")
-    table, blend_w = tables(route_ids, route_weights, tokens.shape[0])
-    new_state, after, packed = mixer(
+    order, share = tables(route_ids, route_weights, tokens.shape[0])
+    new_state, after, packed, blend_w = mixer(
         (tokens, state, norm_gain, w_recept, w_keys, w_values, decay_base, decay_first_matrix,
          decay_second_matrix, rate_base, rate_first_matrix, rate_second_matrix, head_gain,
          w_output, second_gain),
-        table,
+        order,
+        share,
     )
     layer_out = experts(packed, after, blend_w, expert_gate, expert_up, expert_down, devices)
     return (layer_out, new_state)

time: 71.1 us -> 70.1 us (0.986)
  local copies, waits for them, and re-layouts: 3.96 us -> 3.05 us
    eq x4 -> x0, local copies, waits for them, and re-layouts: 0.86 us -> none  [tables(): table = (order == base).astype(F32)]
    convert_element_type x1 -> x0, other arithmetic: 0.77 us -> none  [tables(): table.reshape(flat).astype(BF)]
where the time goes in v3:
time: 70.1 us; the launch traced here: 69.5 us
  Pallas kernels  64.4 us (92%)
  local copies, waits for them, and re-layouts  3.05 us (4%)
  other arithmetic  1.39 us (2%)
    pallas_call x1, Pallas kernels, experts(): pl.pallas_call(functools.partial(expert_kernel, devices), out_shape=jax.S...  37 us
    pallas_call x1, Pallas kernels, mixer(): pl.pallas_call(mixer_kernel, out_shape=(jax.ShapeDtypeStruct(state.shape,...  27.4 us
    unnamed x3, local copies, waits for them, and re-layouts  2.23 us

profile of v3, /device:TPU:0, one launch (start us, length us, event | category | flops | bytes accessed | tf_op | source)
XLA Modules:
  0.0 69.5 jit_solution(17296721655529367562)
XLA Ops:
  0.6 0.0 copy-start
  0.6 0.7 copy-done
  1.3 0.1 constant_dynamic-slice_fusion.1
  1.4 0.8 %constant_dynamic-slice_fusion = f32[24,2]{0,1:T(2,128)S(1)} fusion(f32[768,2]{0,1:T(2,128)} %param.38, s32[]{:T(128)S(6)} %select_n.12), kind=kLoop, calls=%fused_computation.4 | loop fusion | bytes 388 | tf_op jit(solution)/shard_map/dynamic_slice | solution.py:500
  2.2 0.6 select_reduce_fusion.share
  2.8 0.2 reduce_window_sum.11
  2.9 0.6 add_select_fusion.order
  3.6 27.4 %mixer.1 = (f32[24,16,64,64]{3,2,1,0:T(8,128)}, f32[24,2048]{1,0:T(8,128)}, bf16[16,8,1536]{2,1,0:T(8,128)(2,1)}, f32[4,128,24]{2,1,0:T(8,128)}) custom-call(bf16[24,2048]{1,0:T(8,128)(2,1)} %tokens.1, f32[1,2048]{1,0:T(1,128)} %bitcast.5, f32[1,1024]{1,0:T(1,128)} %bitcast.7, f32[1,1024]{1,0:T(1,128)} %bitcast.8, f32[1,1024]{1,0:T(1,128)} %bitcast.9, ...), custom_call_target="tpu_custom_call" | custom-call | tf_op jit(solution)/shard_map/mixer/pallas_call | solution.py:181
  30.9 37.0 %experts.1 = bf16[24,2048]{1,0:T(8,128)(2,1)} custom-call(bf16[16,8,1536]{2,1,0:T(8,128)(2,1)} %get-tuple-element.6.packed, f32[24,2048]{1,0:T(8,128)} %get-tuple-element.7.after, f32[4,128,24]{2,1,0:T(8,128)} %get-tuple-element.8.blend_w, bf16[4,96,128]{2,1,0:T(8,128)(2,1)} %constant.25.clone.unpack_m, bf16[4,128,96]{2,1,0:T(8,128)(2,1)} %constant.26.clone.pack_m, ...), custom_call_target="tpu_custom_call" | custom-call | tf_op jit(solution)/shard_map/experts/pallas_call | solution.py:462
  68.0 1.5 %copy.27 = bf16[24,2048]{1,0:T(8,128)(2,1)} copy(bf16[24,2048]{1,0:T(8,128)(2,1)} %experts.1) | data formatting | bytes 196608
  (2 shorter events, 0.0 us)
Async XLA Ops:
  0.6 0.7 %copy-start = (s32[768,2]{0,1:T(2,128)S(1)}, s32[768,2]{0,1:T(2,128)}, u32[]{:S(2)}) copy-start(s32[768,2]{0,1:T(2,128)} %param.37) | copy-start | bytes 18436
